TPU v7x, 32 devices: a whole 2x2x4 slice. The times are simulated.
32 devices in a mesh: kv: 4 (over y, x), tp: 8 (over z, core).
Axes of the slice: x: 2, y: 2, z: 4, core: 2. Of those that a mesh axis runs over, the one named last changes fastest.
Arguments:
- tokens: bfloat16 [16, 4096], P(None, ('kv', 'tp')), may hold values from -9 to 9
- lengths: int32 [16], replicated, may hold values from 1 to 4096, 16384 in all
- gain_attn: float32 [4096], P('kv'), may hold values from 0.1 to 1.9
- w_query_nope: bfloat16 [4096, 4096], P('kv', 'tp'), may hold values from -0.09375 to 0.09375
- w_query_rope: bfloat16 [4096, 2048], P('kv', 'tp'), may hold values from -0.09375 to 0.09375
- w_latent: bfloat16 [4096, 512], P('kv'), may hold values from -0.09375 to 0.09375
- w_rope_key: bfloat16 [4096, 64], P('kv'), may hold values from -0.09375 to 0.09375
- gain_latent: float32 [512], replicated, may hold values from 0.1 to 1.9
- w_key_up: bfloat16 [512, 4096], P(None, 'tp'), may hold values from -0.75 to 0.75
- w_value_up: bfloat16 [512, 4096], P(None, 'tp'), may hold values from -0.25 to 0.25
- w_out: bfloat16 [4096, 4096], P('tp', 'kv'), may hold values from -0.25 to 0.25
- gain_mlp: float32 [4096], P('kv'), may hold values from 0.1 to 1.9
- w_up: bfloat16 [4096, 16384], P('kv', 'tp'), may hold values from -0.09375 to 0.09375
- w_down: bfloat16 [16384, 4096], P('tp', 'kv'), may hold values from -0.046875 to 0.046875
- cache_latent: bfloat16 [16, 4096, 512], P('tp', 'kv'), may hold values from -6 to 6
- cache_rope: bfloat16 [16, 4096, 64], P('tp', 'kv'), may hold values from -900 to 900
Outputs:
- mixed: bfloat16 [16, 4096], P(None, ('kv', 'tp'))
Inputs may be any that keep to these rules, and one draw needn't show every extreme that they name: `lengths`: one sequence has exactly 4096 live positions.
All inputs are finite; a program needn't handle non-finite values.
Results may differ from a plain program's by a relative error of at most 0.035.
The roundings to bfloat16 on the way count: a program that leaves them out, or rounds other values in their place, can miss the bound.
Values may be sent and summed in bfloat16 or wider, within the bound.
A program may use at most 64 MiB of HBM per device.

v0:
```python
import jax
import jax.numpy as jnp
from jax import lax
from jax.sharding import PartitionSpec as P

D = 4096
NOPE = 128
ROPE = 64
VD = 128
RANK = 512
EPS = 1e-06


def merged_2(value, axis, combine):
    everything = jax.tree.map(
        lambda part, kind: lax.all_gather(part.astype(kind), axis),
        value,
        (jnp.bfloat16, jnp.bfloat16, jnp.bfloat16),
    )

    def take(k):
        return jax.tree.map(lambda part, own: part[k].astype(own.dtype), everything, value)

    return lax.fori_loop(
        1, lax.axis_size(axis), lambda k, so_far: combine(so_far, take(k)), take(0)
    )


def rotate(values, positions):
    half_dim = values.shape[-1] // 2
    inv_freq = 10000.0 ** (-jnp.arange(half_dim, dtype=jnp.float32) / half_dim)
    angles = positions.astype(jnp.float32)[..., None] * inv_freq
    cos_part = jnp.cos(angles)
    sin_part = jnp.sin(angles)
    lower = values[..., :half_dim]
    upper = values[..., half_dim:]
    return jnp.concatenate(
        [lower * cos_part - upper * sin_part, upper * cos_part + lower * sin_part], axis=-1
    )


def combine(earlier, later):
    max_one, sum_one, out_one = earlier
    max_two, sum_two, out_two = later
    new_max = jnp.maximum(max_one, max_two)
    weight_one = sum_one * jnp.exp(max_one - new_max)
    weight_two = sum_two * jnp.exp(max_two - new_max)
    merged = weight_one + weight_two
    safe_sum = jnp.where(merged > 0, merged, 1.0)
    result = (
        weight_one[..., None] * out_one.astype(jnp.float32)
        + weight_two[..., None] * out_two.astype(jnp.float32)
    ) / safe_sum[..., None]
    return (new_max, merged, result.astype(jnp.bfloat16))


def per_device(
    tokens,
    lengths,
    gain_attn,
    w_query_nope,
    w_query_rope,
    w_latent,
    w_rope_key,
    gain_latent,
    w_key_up,
    w_value_up,
    w_out,
    gain_mlp,
    w_up,
    w_down,
    cache_latent,
    cache_rope,
):
    kv_index = lax.axis_index("kv")
    tp_index = lax.axis_index("tp")
    seq_dev = cache_latent.shape[0]
    cache_dev = cache_latent.shape[1]
    heads_dev = w_key_up.shape[1] // NOPE
    block_cols = lax.all_gather(tokens, "tp", axis=1, tiled=True)
    batch_rows = block_cols.shape[0]
    widened = block_cols.astype(jnp.float32)
    square_piece = jnp.sum(widened * widened, axis=1)
    scaled = (widened * gain_attn).astype(jnp.bfloat16)
    part_nope = jnp.dot(scaled, w_query_nope, preferred_element_type=jnp.float32)
    part_rope = jnp.dot(scaled, w_query_rope, preferred_element_type=jnp.float32)
    own_rows = lax.dynamic_slice_in_dim(scaled, tp_index * seq_dev, seq_dev, 0)
    part_latent = jnp.dot(own_rows, w_latent, preferred_element_type=jnp.float32)
    part_key = jnp.dot(own_rows, w_rope_key, preferred_element_type=jnp.float32)
    square_sum, nope_sum, rope_sum, latent_sum, key_sum = lax.psum(
        (square_piece, part_nope, part_rope, part_latent, part_key), "kv"
    )
    inv_rms = lax.rsqrt(square_sum / D + EPS)
    q_nope = (nope_sum * inv_rms[:, None]).astype(jnp.bfloat16).reshape(batch_rows, heads_dev, NOPE)
    rope_raw = (rope_sum * inv_rms[:, None]).reshape(batch_rows, heads_dev, ROPE)
    q_rope = rotate(rope_raw, lengths[:, None]).astype(jnp.bfloat16)
    key_up = w_key_up.reshape(RANK, heads_dev, NOPE)
    q_latent = jnp.einsum(
        "bhn,rhn->bhr", q_nope, key_up, preferred_element_type=jnp.float32
    ).astype(jnp.bfloat16)
    latent_query, rope_query = (
        lax.all_to_all(q_latent, "tp", split_axis=0, concat_axis=1, tiled=True),
        lax.all_to_all(q_rope, "tp", split_axis=0, concat_axis=1, tiled=True),
    )
    own_inv = lax.dynamic_slice_in_dim(inv_rms, tp_index * seq_dev, seq_dev, 0)
    own_len = lax.dynamic_slice_in_dim(lengths, tp_index * seq_dev, seq_dev, 0)
    raw_latent = latent_sum * own_inv[:, None]
    latent_new = (
        raw_latent
        * lax.rsqrt(jnp.mean(raw_latent * raw_latent, axis=1, keepdims=True) + EPS)
        * gain_latent
    ).astype(jnp.bfloat16)
    key_new = rotate(key_sum * own_inv[:, None], own_len).astype(jnp.bfloat16)
    score_scale = (NOPE + ROPE) ** (-0.5)
    positions = kv_index * cache_dev + jnp.arange(cache_dev, dtype=jnp.int32)
    rotated = rotate(cache_rope.astype(jnp.float32), positions).astype(jnp.bfloat16)
    scores = (
        jnp.einsum("shr,spr->shp", latent_query, cache_latent, preferred_element_type=jnp.float32)
        + jnp.einsum("shk,spk->shp", rope_query, rotated, preferred_element_type=jnp.float32)
    ) * score_scale
    live_mask = positions[None, None, :] < own_len[:, None, None]
    block_max = jnp.max(jnp.where(live_mask, scores, -1e30), axis=2)
    exponent = jnp.where(live_mask, jnp.exp(scores - block_max[..., None]), 0.0)
    block_sum = jnp.sum(exponent, axis=2)
    weighted = jnp.einsum(
        "shp,spr->shr",
        exponent.astype(jnp.bfloat16),
        cache_latent,
        preferred_element_type=jnp.float32,
    )
    block_out = (weighted / jnp.where(block_sum > 0, block_sum, 1.0)[..., None]).astype(
        jnp.bfloat16
    )
    block_max, block_sum, block_out = merged_2((block_max, block_sum, block_out), "kv", combine)
    own_score = (
        jnp.einsum("shr,sr->sh", latent_query, latent_new, preferred_element_type=jnp.float32)
        + jnp.einsum("shk,sk->sh", rope_query, key_new, preferred_element_type=jnp.float32)
    ) * score_scale
    new_max = jnp.maximum(block_max, own_score)
    carried = block_sum * jnp.exp(block_max - new_max)
    own_weight = jnp.exp(own_score - new_max)
    o_latent = (
        (
            carried[..., None] * block_out.astype(jnp.float32)
            + own_weight[..., None] * latent_new.astype(jnp.float32)[:, None, :]
        )
        / (carried + own_weight)[..., None]
    ).astype(jnp.bfloat16)
    head_latent = lax.all_to_all(o_latent, "tp", split_axis=1, concat_axis=0, tiled=True)
    value_up = w_value_up.reshape(RANK, heads_dev, VD)
    head_out = (
        jnp.einsum("bhr,rhv->bhv", head_latent, value_up, preferred_element_type=jnp.float32)
        .astype(jnp.bfloat16)
        .reshape(batch_rows, heads_dev * VD)
    )
    attn_part = jnp.dot(head_out, w_out, preferred_element_type=jnp.float32)
    attn_sum = lax.psum(attn_part, "tp")
    resid = (widened + attn_sum).astype(jnp.bfloat16)
    resid_wide = resid.astype(jnp.float32)
    square_two = jnp.sum(resid_wide * resid_wide, axis=1)
    scaled2 = (resid_wide * gain_mlp).astype(jnp.bfloat16)
    up_part = jnp.dot(scaled2, w_up, preferred_element_type=jnp.float32)
    spread_squares = jnp.broadcast_to(square_two[:, None], (batch_rows, lax.axis_size("kv")))
    up_share, square_cols = (
        lax.psum_scatter(up_part, "kv", scatter_dimension=1, tiled=True),
        lax.psum_scatter(spread_squares, "kv", scatter_dimension=1, tiled=True),
    )
    square_all = square_cols[:, 0]
    active_share = jnp.square(jnp.maximum(up_share, 0.0)).astype(jnp.bfloat16)
    activated = lax.all_gather(active_share, "kv", axis=1, tiled=True)
    inv_rms2 = lax.rsqrt(square_all / D + EPS)
    down_part = jnp.dot(activated, w_down, preferred_element_type=jnp.float32)
    down_sum = lax.psum_scatter(down_part, "tp", scatter_dimension=1, tiled=True)
    out_cols = down_sum.shape[1]
    resid_cols = lax.dynamic_slice_in_dim(resid_wide, tp_index * out_cols, out_cols, 1)
    return (resid_cols + (inv_rms2 * inv_rms2)[:, None] * down_sum).astype(jnp.bfloat16)


def solution(mesh):
    in_specs = (
        P(None, ("kv", "tp")),
        P(),
        P("kv"),
        P("kv", "tp"),
        P("kv", "tp"),
        P("kv", None),
        P("kv", None),
        P(),
        P(None, "tp"),
        P(None, "tp"),
        P("tp", "kv"),
        P("kv"),
        P("kv", "tp"),
        P("tp", "kv"),
        P("tp", "kv", None),
        P("tp", "kv", None),
    )
    out_specs = P(None, ("kv", "tp"))
    return jax.shard_map(
        per_device, mesh=mesh, in_specs=in_specs, out_specs=out_specs, check_vma=False
    )
```

profile of v0, /device:TPU:0, one launch (start us, length us, event | category | flops | bytes accessed | tf_op | source)
XLA Modules:
  0.0 232.3 jit_solution(9144840730613302866)
XLA Ops:
  7.4 14.6 %all_gather.20 = bf16[16,1024]{1,0:T(8,128)(2,1)S(1)} all-gather(bf16[16,128]{1,0:T(8,128)(2,1)} %param.18), channel_id=1, replica_groups=mesh['kv'=4,'tp'=8] {'tp'}, dimensions={1}, use_global_device_ids=true | all-gather | bytes 36864 | tf_op jit(solution)/shard_map/all_gather | solution.py:80
  22.8 1.0 fusion.39
  23.8 1.5 fusion.41
  25.3 1.2 fusion.73
  26.5 1.5 fusion.71
  28.0 17.0 %all-reduce.1 = (f32[16,512]{1,0:T(8,128)S(1)}, f32[16]{0:T(128)S(1)}, f32[16,256]{1,0:T(8,128)S(1)}, f32[2,512]{1,0:T(2,128)S(1)}, f32[2,64]{1,0:T(2,128)S(1)}) all-reduce(f32[16,512]{1,0:T(8,128)S(1)} %fusion.71, f32[16]{0:T(128)S(1)} %get-tuple-element.223, f32[16,256]{1,0:T(8,128)S(1)} %fusion.73, ...), channel_id=1, replica_groups=mesh['kv'=4,'tp'=8] {'kv'}, use_global_device_ids=true, to_apply=%region_0.0 | all-reduce | flops 13456 | bytes 107648 | tf_op jit(solution)/shard_map/psum | solution.py:90
  46.2 3.4 %all-to-all-start.1 = ((bf16[8,2,256]{2,1,0:T(2,128)(2,1)}), bf16[8,2,256]{2,1,0:T(2,128)(2,1)S(1)}, u32[]{:S(2)}, u32[]{:S(2)}) async-start(bf16[8,2,256]{2,1,0:T(2,128)(2,1)} %reshape.265), calls=%async_computation.1 | async-start | bytes 16384 | tf_op jit(solution)/shard_map/all_to_all | solution.py:103
  51.2 1.0 convert_element_type.177
  53.6 1.6 all-to-all-done.1
  55.2 3.5 %all-to-all-start = ((bf16[16,4,512]{2,1,0:T(4,128)(2,1)}), bf16[16,4,512]{2,1,0:T(4,128)(2,1)S(1)}, u32[]{:S(2)}, u32[]{:S(2)}) async-start(bf16[16,4,512]{2,1,0:T(4,128)(2,1)} %copy.32), calls=%async_computation | async-start | bytes 131072 | tf_op jit(solution)/shard_map/all_to_all | solution.py:102
  59.0 5.7 %all-to-all-done = bf16[16,4,512]{2,1,0:T(4,128)(2,1)S(1)} async-done(((bf16[16,4,512]{2,1,0:T(4,128)(2,1)}), bf16[16,4,512]{2,1,0:T(4,128)(2,1)S(1)}, u32[]{:S(2)}, u32[]{:S(2)}) %all-to-all-start) | async-done | bytes 65568 | tf_op jit(solution)/shard_map/all_to_all | solution.py:102
  66.5 7.1 %all-gather.3 = bf16[4,2,32]{2,1,0:T(2,128)(2,1)S(1)} all-gather(bf16[1,2,32]{2,1,0:T(2,128)(2,1)S(1)} %convert_bitcast_fusion.1), channel_id=2, replica_groups=mesh['kv'=4,'tp'=8] {'kv'}, dimensions={0}, use_global_device_ids=true | all-gather | bytes 640 | tf_op jit(solution)/shard_map/all_gather | solution.py:16
  73.7 7.8 %all-gather.4 = bf16[4,2,32]{2,1,0:T(2,128)(2,1)S(1)} all-gather(bf16[1,2,32]{2,1,0:T(2,128)(2,1)S(1)} %get-tuple-element.230), channel_id=3, replica_groups=mesh['kv'=4,'tp'=8] {'kv'}, dimensions={0}, use_global_device_ids=true | all-gather | bytes 640 | tf_op jit(solution)/shard_map/all_gather | solution.py:16
  81.4 8.1 %all-gather.2 = bf16[8,32,512]{2,1,0:T(8,128)(2,1)S(1)} all-gather(bf16[2,32,512]{2,1,0:T(8,128)(2,1)S(1)} %fusion.8), channel_id=4, replica_groups=mesh['kv'=4,'tp'=8] {'kv'}, dimensions={0}, use_global_device_ids=true | all-gather | bytes 327680 | tf_op jit(solution)/shard_map/all_gather | solution.py:16
  90.5 8.3 %all_to_all.54 = bf16[2,32,512]{2,0,1:T(2,128)(2,1)S(1)} all-to-all(bf16[2,32,512]{2,0,1:T(2,128)(2,1)S(1)} %fusion.21), channel_id=1, replica_groups=mesh['kv'=4,'tp'=8] {'tp'}, dimensions={1} | all-to-all | bytes 131072 | tf_op jit(solution)/shard_map/all_to_all | solution.py:149
  98.9 1.2 fusion.10
  101.1 52.4 %all-reduce.4.cloned.1.call-done = f32[16,1024]{1,0:T(8,128)} async-done(((f32[16,1024]{1,0:T(8,128)}), f32[16,1024]{1,0:T(8,128)}) %all-reduce.4.cloned.1.call-update) | async-done | bytes 65552 | tf_op jit(solution)/shard_map/psum | solution.py:157
  154.5 3.5 %fusion.28 = f32[16,2048]{1,0:T(8,128)} fusion(bf16[1024,2048]{1,0:T(8,128)(2,1)} %param.30, f32[16,1024]{1,0:T(8,128)S(1)} %get-tuple-element.211, f32[1024]{0:T(1024)S(1)} %copy-done.3), kind=kOutput, calls=%fused_computation.52 | convolution fusion | flops 67141632 | bytes 4395008 | tf_op jit(solution)/shard_map/dot_general | solution.py:162
  158.0 23.3 %reduce-scatter.3.cloned.1.call-done = f32[16,512]{1,0:T(8,128)} async-done(((f32[16,2048]{1,0:T(8,128)}), f32[16,512]{1,0:T(8,128)}) %reduce-scatter.3.cloned.1.call-update) | async-done | bytes 32784 | tf_op jit(solution)/shard_map/reduce_scatter | solution.py:165
  182.1 8.2 %all_gather.25 = bf16[16,2048]{1,0:T(8,128)(2,1)S(1)} all-gather(bf16[16,512]{1,0:T(8,128)(2,1)S(1)} %multiply_convert_fusion.2), channel_id=1, replica_groups=mesh['kv'=4,'tp'=8] {'kv'}, dimensions={1}, use_global_device_ids=true | all-gather | bytes 81920 | tf_op jit(solution)/shard_map/all_gather | solution.py:170
  190.3 3.5 %fusion.74 = f32[16,1024]{1,0:T(8,128)} fusion(bf16[16,2048]{1,0:T(8,128)(2,1)S(1)} %all_gather.25, bf16[2048,1024]{1,0:T(8,128)(2,1)} %param.31), kind=kOutput, calls=%fused_computation.124 | convolution fusion | flops 67108864 | bytes 4325376 | tf_op jit(solution)/shard_map/dot_general | solution.py:172
  194.4 8.9 %all-reduce = f32[16,4]{0,1:T(4,128)S(1)} all-reduce(f32[16,4]{0,1:T(4,128)S(1)} %broadcast_in_dim.47), channel_id=5, replica_groups=mesh['kv'=4,'tp'=8] {'kv'}, use_global_device_ids=true, to_apply=%region_13.14.clone | all-reduce | flops 64 | bytes 512
  204.0 20.4 %reduce-scatter.5.cloned.1.call-done = f32[16,128]{1,0:T(8,128)} async-done(((f32[16,1024]{1,0:T(8,128)}), f32[16,128]{1,0:T(8,128)}) %reduce-scatter.5.cloned.1.call-update) | async-done | bytes 8208 | tf_op jit(solution)/shard_map/reduce_scatter | solution.py:173
  224.4 1.4 add_convert_fusion.2
  (77 shorter events, 13.3 us)
Async XLA Ops:
  6.5 58.3 %copy-start = (bf16[2,1024,512]{2,1,0:T(8,128)(2,1)S(1)}, bf16[2,1024,512]{2,1,0:T(8,128)(2,1)}, u32[]{:S(2)}) copy-start(bf16[2,1024,512]{2,1,0:T(8,128)(2,1)} %param.32) | copy-start | bytes 6291460
  6.5 45.9 %copy-start.4 = (f32[512]{0:T(512)S(1)}, f32[512]{0:T(512)}, u32[]{:S(2)}) copy-start(f32[512]{0:T(512)} %param.25) | copy-start | bytes 6148
  6.5 46.0 %copy-start.2 = (bf16[512,512]{1,0:T(8,128)(2,1)S(1)}, bf16[512,512]{1,0:T(8,128)(2,1)}, u32[]{:S(2)}) copy-start(bf16[512,512]{1,0:T(8,128)(2,1)} %param.26) | copy-start | bytes 1572868
  46.2 9.0 %all-to-all-start.1 = ((bf16[8,2,256]{2,1,0:T(2,128)(2,1)}), bf16[8,2,256]{2,1,0:T(2,128)(2,1)S(1)}, u32[]{:S(2)}, u32[]{:S(2)}) async-start(bf16[8,2,256]{2,1,0:T(2,128)(2,1)} %reshape.265), calls=%async_computation.1 | async-start | bytes 16384 | tf_op jit(solution)/shard_map/all_to_all | solution.py:103
  55.2 9.4 %all-to-all-start = ((bf16[16,4,512]{2,1,0:T(4,128)(2,1)}), bf16[16,4,512]{2,1,0:T(4,128)(2,1)S(1)}, u32[]{:S(2)}, u32[]{:S(2)}) async-start(bf16[16,4,512]{2,1,0:T(4,128)(2,1)} %copy.32), calls=%async_computation | async-start | bytes 131072 | tf_op jit(solution)/shard_map/all_to_all | solution.py:102
  58.7 94.8 %all-reduce.4.cloned.1.call-start = ((), (), s32[]{:S(2)}) async-start(), calls=%async_computation.5 | async-start | bytes 131072 | tf_op jit(solution)/shard_map/psum | solution.py:157
  64.8 35.3 %copy-start.1 = (bf16[512,1024]{1,0:T(8,128)(2,1)S(1)}, bf16[512,1024]{1,0:T(8,128)(2,1)}, u32[]{:S(2)}) copy-start(bf16[512,1024]{1,0:T(8,128)(2,1)} %param.28) | copy-start | bytes 3145732
  65.5 88.9 %copy-start.3 = (f32[1024]{0:T(1024)S(1)}, f32[1024]{0:T(1024)}, u32[]{:S(2)}) copy-start(f32[1024]{0:T(1024)} %param.29) | copy-start | bytes 12292
  101.1 80.3 %reduce-scatter.3.cloned.1.call-start = ((), (), s32[]{:S(2)}) async-start(), calls=%async_computation.6 | async-start | bytes 163840 | tf_op jit(solution)/shard_map/reduce_scatter | solution.py:165
  154.5 39.3 %copy-start.5 = (u32[32]{0:T(128)S(1)}, u32[32]{0:T(128)}, u32[]{:S(2)}) copy-start(u32[32]{0:T(128)} %constant.104) | copy-start | bytes 388
  158.0 66.4 %reduce-scatter.5.cloned.1.call-start = ((), (), s32[]{:S(2)}) async-start(), calls=%async_computation.7 | async-start | bytes 73728 | tf_op jit(solution)/shard_map/reduce_scatter | solution.py:173
Sparse Core Ops, SparseCore 0:
  101.2 52.2 all-reduce.3
  158.1 23.2 reduce-scatter.2
  193.9 30.4 reduce-scatter.4
where the time goes:
time: 233 us; the launch traced here: 232 us
  waiting for transfers between devices  103 us (44%)
  blocking collectives  80 us (34%)
  matrix products  16.3 us (7%)
  between operations  13.3 us (6%)
  other arithmetic  9.51 us (4%)
  starting transfers between devices  7.03 us (3%)
  local copies, waits for them, and re-layouts  2.62 us (1%)
    psum x1, waiting for transfers between devices, per_device(): attn_sum = lax.psum(attn_part, 'tp')  52.4 us
    reduce_scatter x1, waiting for transfers between devices, per_device(): lax.psum_scatter(up_part, 'kv', scatter_dimension=1, tiled=True)  23.3 us
    all_gather x3, blocking collectives, merged_2(): lax.all_gather(part.astype(kind), axis)  23 us
    reduce_scatter x1, waiting for transfers between devices, per_device(): lax.psum_scatter(down_part, 'tp', scatter_dimension=1, tiled=True)  20.4 us
    psum x1, blocking collectives, per_device(): lax.psum((square_piece, part_nope, part_rope, part_latent, part_key), 'kv')  17 us
    all_gather x1, blocking collectives, per_device(): block_cols = lax.all_gather(tokens, 'tp', axis=1, tiled=True)  14.6 us
    unnamed x1, blocking collectives  8.89 us
    all_to_all x1, blocking collectives, per_device(): lax.all_to_all(o_latent, 'tp', split_axis=1, concat_axis=0, tiled=True)  8.3 us
  transfers between devices with their start and end apart: 5, of which 5 were waited for; matrix products, arithmetic and copies ran while one was open for 2% of the time, Pallas kernels for 0%

commit v1 on v0

--- a/solution.py
+++ b/solution.py
@@ -154,7 +154,7 @@
         .reshape(batch_rows, heads_dev * VD)
     )
     attn_part = jnp.dot(head_out, w_out, preferred_element_type=jnp.float32)
-    attn_sum = lax.psum(attn_part, "tp")
+    attn_sum = jnp.sum(lax.all_gather(attn_part, "tp"), axis=0)
     resid = (widened + attn_sum).astype(jnp.bfloat16)
     resid_wide = resid.astype(jnp.float32)
     square_two = jnp.sum(resid_wide * resid_wide, axis=1)

time: 233 us -> 193 us (0.83)
  waiting for transfers between devices: 103 us -> 49.4 us
  blocking collectives: 80 us -> 94.8 us
    psum x1 -> x0, waiting for transfers between devices: 52.4 us -> none  [per_device(): attn_sum = lax.psum(attn_part, 'tp')]
    all_gather x0 -> x1, blocking collectives: none -> 14.8 us  [per_device(): attn_sum = jnp.sum(lax.all_gather(attn_part, 'tp'), axis=0)]
  transfers between devices with their start and end apart: 5 -> 4, of which waited for: 5 -> 4; matrix products, arithmetic and copies ran while one was open for 2% -> 3% of each run, Pallas kernels for 0% -> 0%
where the time goes in v1:
time: 193 us; the launch traced here: 192 us
  blocking collectives  94.8 us (49%)
  waiting for transfers between devices  49.4 us (26%)
  matrix products  15.7 us (8%)
  between operations  13.6 us (7%)
  other arithmetic  8.69 us (5%)
  starting transfers between devices  6.99 us (4%)
  local copies, waits for them, and re-layouts  2.62 us (1%)
    all_gather x3, blocking collectives, merged_2(): lax.all_gather(part.astype(kind), axis)  23 us
    reduce_scatter x1, waiting for transfers between devices, per_device(): lax.psum_scatter(up_part, 'kv', scatter_dimension=1, tiled=True)  21.7 us
    reduce_scatter x1, waiting for transfers between devices, per_device(): lax.psum_scatter(down_part, 'tp', scatter_dimension=1, tiled=True)  20.5 us
    psum x1, blocking collectives, per_device(): lax.psum((square_piece, part_nope, part_rope, part_latent, part_key), 'kv')  17 us
    all_gather x1, blocking collectives, per_device(): attn_sum = jnp.sum(lax.all_gather(attn_part, 'tp'), axis=0)  14.8 us
    all_gather x1, blocking collectives, per_device(): block_cols = lax.all_gather(tokens, 'tp', axis=1, tiled=True)  14.6 us
    unnamed x1, blocking collectives  8.89 us
    all_to_all x1, blocking collectives, per_device(): lax.all_to_all(o_latent, 'tp', split_axis=1, concat_axis=0, tiled=True)  8.3 us
  transfers between devices with their start and end apart: 4, of which 4 were waited for; matrix products, arithmetic and copies ran while one was open for 3% of the time, Pallas kernels for 0%

profile of v1, /device:TPU:0, one launch (start us, length us, event | category | flops | bytes accessed | tf_op | source)
XLA Modules:
  0.0 191.9 jit_solution(16051892422470495292)
XLA Ops:
  7.4 14.6 %all_gather.26 = bf16[16,1024]{1,0:T(8,128)(2,1)S(1)} all-gather(bf16[16,128]{1,0:T(8,128)(2,1)} %param.18), channel_id=1, replica_groups=mesh['kv'=4,'tp'=8] {'tp'}, dimensions={1}, use_global_device_ids=true | all-gather | bytes 36864 | tf_op jit(solution)/shard_map/all_gather | solution.py:80
  22.8 1.0 fusion.39
  23.8 1.5 fusion.41
  25.3 1.2 fusion.73
  26.5 1.5 fusion.71
  28.0 17.0 %all-reduce.1 = (f32[16,512]{1,0:T(8,128)S(1)}, f32[16]{0:T(128)S(1)}, f32[16,256]{1,0:T(8,128)S(1)}, f32[2,512]{1,0:T(2,128)S(1)}, f32[2,64]{1,0:T(2,128)S(1)}) all-reduce(f32[16,512]{1,0:T(8,128)S(1)} %fusion.71, f32[16]{0:T(128)S(1)} %get-tuple-element.223, f32[16,256]{1,0:T(8,128)S(1)} %fusion.73, ...), channel_id=1, replica_groups=mesh['kv'=4,'tp'=8] {'kv'}, use_global_device_ids=true, to_apply=%region_0.0 | all-reduce | flops 13456 | bytes 107648 | tf_op jit(solution)/shard_map/psum | solution.py:90
  46.2 3.4 %all-to-all-start.1 = ((bf16[8,2,256]{2,1,0:T(2,128)(2,1)}), bf16[8,2,256]{2,1,0:T(2,128)(2,1)S(1)}, u32[]{:S(2)}, u32[]{:S(2)}) async-start(bf16[8,2,256]{2,1,0:T(2,128)(2,1)} %reshape.266), calls=%async_computation.1 | async-start | bytes 16384 | tf_op jit(solution)/shard_map/all_to_all | solution.py:103
  51.2 1.0 convert_element_type.177
  53.6 1.6 all-to-all-done.1
  55.2 3.5 %all-to-all-start = ((bf16[16,4,512]{2,1,0:T(4,128)(2,1)}), bf16[16,4,512]{2,1,0:T(4,128)(2,1)S(1)}, u32[]{:S(2)}, u32[]{:S(2)}) async-start(bf16[16,4,512]{2,1,0:T(4,128)(2,1)} %copy.32), calls=%async_computation | async-start | bytes 131072 | tf_op jit(solution)/shard_map/all_to_all | solution.py:102
  59.0 5.7 %all-to-all-done = bf16[16,4,512]{2,1,0:T(4,128)(2,1)S(1)} async-done(((bf16[16,4,512]{2,1,0:T(4,128)(2,1)}), bf16[16,4,512]{2,1,0:T(4,128)(2,1)S(1)}, u32[]{:S(2)}, u32[]{:S(2)}) %all-to-all-start) | async-done | bytes 65568 | tf_op jit(solution)/shard_map/all_to_all | solution.py:102
  66.5 7.1 %all-gather.4 = bf16[4,2,32]{2,1,0:T(2,128)(2,1)S(1)} all-gather(bf16[1,2,32]{2,1,0:T(2,128)(2,1)S(1)} %convert_bitcast_fusion.1), channel_id=2, replica_groups=mesh['kv'=4,'tp'=8] {'kv'}, dimensions={0}, use_global_device_ids=true | all-gather | bytes 640 | tf_op jit(solution)/shard_map/all_gather | solution.py:16
  73.7 7.8 %all-gather.5 = bf16[4,2,32]{2,1,0:T(2,128)(2,1)S(1)} all-gather(bf16[1,2,32]{2,1,0:T(2,128)(2,1)S(1)} %get-tuple-element.230), channel_id=3, replica_groups=mesh['kv'=4,'tp'=8] {'kv'}, dimensions={0}, use_global_device_ids=true | all-gather | bytes 640 | tf_op jit(solution)/shard_map/all_gather | solution.py:16
  81.4 8.1 %all-gather.2 = bf16[8,32,512]{2,1,0:T(8,128)(2,1)S(1)} all-gather(bf16[2,32,512]{2,1,0:T(8,128)(2,1)S(1)} %fusion.8), channel_id=4, replica_groups=mesh['kv'=4,'tp'=8] {'kv'}, dimensions={0}, use_global_device_ids=true | all-gather | bytes 327680 | tf_op jit(solution)/shard_map/all_gather | solution.py:16
  90.5 8.3 %all_to_all.54 = bf16[2,32,512]{2,0,1:T(2,128)(2,1)S(1)} all-to-all(bf16[2,32,512]{2,0,1:T(2,128)(2,1)S(1)} %fusion.21), channel_id=1, replica_groups=mesh['kv'=4,'tp'=8] {'tp'}, dimensions={1} | all-to-all | bytes 131072 | tf_op jit(solution)/shard_map/all_to_all | solution.py:149
  98.9 1.2 fusion.10
  100.4 14.8 %all-gather.3 = f32[128,1024]{1,0:T(8,128)S(1)} all-gather(f32[16,1024]{1,0:T(8,128)S(1)} %fusion.32), channel_id=5, replica_groups=mesh['kv'=4,'tp'=8] {'tp'}, dimensions={0}, use_global_device_ids=true | all-gather | bytes 589824 | tf_op jit(solution)/shard_map/all_gather | solution.py:157
  115.4 3.5 %fusion.28 = f32[16,2048]{1,0:T(8,128)} fusion(bf16[1024,2048]{1,0:T(8,128)(2,1)} %param.30, f32[16,1024]{1,0:T(8,128)S(1)} %get-tuple-element.211, f32[1024]{0:T(1024)S(1)} %copy-done.3), kind=kOutput, calls=%fused_computation.52 | convolution fusion | flops 67141632 | bytes 4395008 | tf_op jit(solution)/shard_map/dot_general | solution.py:162
  119.0 21.7 %reduce-scatter.3.cloned.1.call-done = f32[16,512]{1,0:T(8,128)} async-done(((f32[16,2048]{1,0:T(8,128)}), f32[16,512]{1,0:T(8,128)}) %reduce-scatter.3.cloned.1.call-update) | async-done | bytes 32784 | tf_op jit(solution)/shard_map/reduce_scatter | solution.py:165
  141.4 8.2 %all_gather.33 = bf16[16,2048]{1,0:T(8,128)(2,1)S(1)} all-gather(bf16[16,512]{1,0:T(8,128)(2,1)S(1)} %multiply_convert_fusion.2), channel_id=1, replica_groups=mesh['kv'=4,'tp'=8] {'kv'}, dimensions={1}, use_global_device_ids=true | all-gather | bytes 81920 | tf_op jit(solution)/shard_map/all_gather | solution.py:170
  149.6 3.5 %fusion.74 = f32[16,1024]{1,0:T(8,128)} fusion(bf16[16,2048]{1,0:T(8,128)(2,1)S(1)} %all_gather.33, bf16[2048,1024]{1,0:T(8,128)(2,1)} %param.31), kind=kOutput, calls=%fused_computation.124 | convolution fusion | flops 67108864 | bytes 4325376 | tf_op jit(solution)/shard_map/dot_general | solution.py:172
  153.7 8.9 %all-reduce = f32[16,4]{0,1:T(4,128)S(1)} all-reduce(f32[16,4]{0,1:T(4,128)S(1)} %broadcast_in_dim.47), channel_id=6, replica_groups=mesh['kv'=4,'tp'=8] {'kv'}, use_global_device_ids=true, to_apply=%region_13.14.clone | all-reduce | flops 64 | bytes 512
  163.2 20.5 %reduce-scatter.5.cloned.1.call-done = f32[16,128]{1,0:T(8,128)} async-done(((f32[16,1024]{1,0:T(8,128)}), f32[16,128]{1,0:T(8,128)}) %reduce-scatter.5.cloned.1.call-update) | async-done | bytes 8208 | tf_op jit(solution)/shard_map/reduce_scatter | solution.py:173
  183.7 1.4 add_convert_fusion.2
  (76 shorter events, 11.8 us)
Async XLA Ops:
  6.5 58.3 %copy-start = (bf16[2,1024,512]{2,1,0:T(8,128)(2,1)S(1)}, bf16[2,1024,512]{2,1,0:T(8,128)(2,1)}, u32[]{:S(2)}) copy-start(bf16[2,1024,512]{2,1,0:T(8,128)(2,1)} %param.32) | copy-start | bytes 6291460
  6.5 45.9 %copy-start.4 = (f32[512]{0:T(512)S(1)}, f32[512]{0:T(512)}, u32[]{:S(2)}) copy-start(f32[512]{0:T(512)} %param.25) | copy-start | bytes 6148
  6.5 46.0 %copy-start.2 = (bf16[512,512]{1,0:T(8,128)(2,1)S(1)}, bf16[512,512]{1,0:T(8,128)(2,1)}, u32[]{:S(2)}) copy-start(bf16[512,512]{1,0:T(8,128)(2,1)} %param.26) | copy-start | bytes 1572868
  46.2 9.0 %all-to-all-start.1 = ((bf16[8,2,256]{2,1,0:T(2,128)(2,1)}), bf16[8,2,256]{2,1,0:T(2,128)(2,1)S(1)}, u32[]{:S(2)}, u32[]{:S(2)}) async-start(bf16[8,2,256]{2,1,0:T(2,128)(2,1)} %reshape.266), calls=%async_computation.1 | async-start | bytes 16384 | tf_op jit(solution)/shard_map/all_to_all | solution.py:103
  55.2 9.4 %all-to-all-start = ((bf16[16,4,512]{2,1,0:T(4,128)(2,1)}), bf16[16,4,512]{2,1,0:T(4,128)(2,1)S(1)}, u32[]{:S(2)}, u32[]{:S(2)}) async-start(bf16[16,4,512]{2,1,0:T(4,128)(2,1)} %copy.32), calls=%async_computation | async-start | bytes 131072 | tf_op jit(solution)/shard_map/all_to_all | solution.py:102
  58.7 81.9 %reduce-scatter.3.cloned.1.call-start = ((), (), s32[]{:S(2)}) async-start(), calls=%async_computation.5 | async-start | bytes 163840 | tf_op jit(solution)/shard_map/reduce_scatter | solution.py:165
  64.8 35.3 %copy-start.1 = (bf16[512,1024]{1,0:T(8,128)(2,1)S(1)}, bf16[512,1024]{1,0:T(8,128)(2,1)}, u32[]{:S(2)}) copy-start(bf16[512,1024]{1,0:T(8,128)(2,1)} %param.28) | copy-start | bytes 3145732
  65.8 49.6 %copy-start.3 = (f32[1024]{0:T(1024)S(1)}, f32[1024]{0:T(1024)}, u32[]{:S(2)}) copy-start(f32[1024]{0:T(1024)} %param.29) | copy-start | bytes 12292
  115.4 37.7 %copy-start.5 = (u32[32]{0:T(128)S(1)}, u32[32]{0:T(128)}, u32[]{:S(2)}) copy-start(u32[32]{0:T(128)} %constant.104) | copy-start | bytes 388
  118.9 64.8 %reduce-scatter.5.cloned.1.call-start = ((), (), s32[]{:S(2)}) async-start(), calls=%async_computation.6 | async-start | bytes 73728 | tf_op jit(solution)/shard_map/reduce_scatter | solution.py:173
Sparse Core Ops, SparseCore 0:
  119.1 21.5 reduce-scatter.2
  153.2 30.4 reduce-scatter.4
